TPU v7x, 32 devices: a whole 2x2x4 slice. The times are simulated.
32 devices in a mesh: sp: 8 (over z, x), tp: 4 (over y, core).
Axes of the slice: x: 2, y: 2, z: 4, core: 2. Of those that a mesh axis runs over, the one named last changes fastest.
Arguments:
- queries: bfloat16 [6144, 2048], P('sp', 'tp'), may hold values from -110 to 110
- key_rows: bfloat16 [6144, 512], P('sp', 'tp'), may hold values from -4.5 to 4.5
- values: bfloat16 [6144, 512], P('sp', 'tp'), may hold values from -6 to 6
- sink_logits: float32 [32], P('tp'), may hold values from 2 to 7
- doc_ids: int32 [6144], P('sp'), may hold values from 0 to 3, as said below
- residual: bfloat16 [6144, 2048], P('sp'), may hold values from -20 to 20
- w_out: bfloat16 [2048, 2048], P('tp'), may hold values from -2.390625 to 2.390625
- norm_gain: float32 [2048], replicated, may hold values from 0.1 to 1.9
- w_value_up: bfloat16 [2048, 5632], P('sp', 'tp'), may hold values from -0.125 to 0.125
- w_gate_up: bfloat16 [2048, 5632], P('sp', 'tp'), may hold values from -0.125 to 0.125
- conv_taps: bfloat16 [3, 5632], P(None, 'tp'), may hold values from -3.5 to 3.5
- w_down_t: bfloat16 [2048, 5632], P('sp', 'tp'), may hold values from -0.078125 to 0.078125
Outputs:
- layer_out: bfloat16 [6144, 2048], P('sp', 'tp')
Inputs may be any that keep to these rules, and one draw needn't show every extreme that they name: `doc_ids`: document numbers never fall along the sequence and every one of the 4 documents is present; each document has 2 or more positions.
All inputs are finite; a program needn't handle non-finite values.
Results may differ from a plain program's by a relative error of at most 0.017.
Values may be sent and summed in bfloat16 or wider, within the bound.
A program may use at most 64 MiB of HBM per device.

v0:
```python
import jax
import jax.numpy as jnp
from jax import lax
from jax.sharding import PartitionSpec as P

HEAD_DIM = 64
WINDOW = 128
EPS = 1e-06
NEG = -1e30


def extended(block, sides, width):
    for axis, dim in sides:
        count = lax.axis_size(axis)
        forward = [(i, i + 1) for i in range(count - 1)]
        backward = [(target, source) for source, target in forward]
        low = lax.ppermute(
            lax.slice_in_dim(block, block.shape[dim] - width, None, axis=dim), axis, forward
        )
        high = lax.ppermute(lax.slice_in_dim(block, 0, width, axis=dim), axis, backward)
        block = jnp.concatenate([low, block, high], axis=dim)
    return block


def local_attention(queries, rim_kv, rim_labels, labels, sink_logits, kv_cols):
    rows_here = queries.shape[0]
    blocks = rows_here // WINDOW
    kv_local = kv_cols // HEAD_DIM
    heads_here = queries.shape[1] // HEAD_DIM
    per_kv = heads_here // kv_local
    kv_blocks = rim_kv.reshape(blocks + 2, WINDOW, rim_kv.shape[1])
    kv_window = jnp.concatenate([kv_blocks[:-2], kv_blocks[1:-1], kv_blocks[2:]], axis=1)
    lab_blocks = rim_labels.reshape(blocks + 2, WINDOW)
    doc_window = jnp.concatenate([lab_blocks[:-2], lab_blocks[1:-1], lab_blocks[2:]], axis=1)
    q_blocks = queries.reshape(blocks, WINDOW, kv_local, per_kv, HEAD_DIM)
    k_blocks = kv_window[:, :, :kv_cols].reshape(blocks, 3 * WINDOW, kv_local, HEAD_DIM)
    v_blocks = kv_window[:, :, kv_cols:].reshape(blocks, 3 * WINDOW, kv_local, HEAD_DIM)
    score = jnp.einsum(
        "nqkgd,njkd->nkgqj", q_blocks, k_blocks, preferred_element_type=jnp.float32
    ) * HEAD_DIM ** (-0.5)
    offsets = jnp.arange(3 * WINDOW)[None, :] - WINDOW - jnp.arange(WINDOW)[:, None]
    in_band = jnp.abs(offsets) <= WINDOW
    doc_query = labels.reshape(blocks, WINDOW)
    allowed = in_band[None] & (doc_query[:, :, None] == doc_window[:, None, :])
    allowed = allowed[:, None, None, :, :]
    sink_grid = sink_logits.reshape(kv_local, per_kv)[None, :, :, None]
    highest = jnp.maximum(jnp.max(jnp.where(allowed, score, NEG), axis=-1), sink_grid)
    raw = jnp.where(allowed, jnp.exp(score - highest[..., None]), 0.0)
    total = jnp.sum(raw, axis=-1) + jnp.exp(sink_grid - highest)
    probs = (raw / total[..., None]).astype(jnp.bfloat16)
    attended = jnp.einsum("nkgqj,njkd->nqkgd", probs, v_blocks, preferred_element_type=jnp.float32)
    return attended.reshape(rows_here, queries.shape[1]).astype(jnp.bfloat16)


def per_device(
    queries,
    key_rows,
    values,
    sink_logits,
    doc_ids,
    residual,
    w_out,
    norm_gain,
    w_value_up,
    w_gate_up,
    conv_taps,
    w_down_t,
):
    rows_here = queries.shape[0]
    model_width = residual.shape[1]
    span_cols = model_width // lax.axis_size("tp")
    first_col = lax.axis_index("tp") * span_cols
    kv_cols = key_rows.shape[1]
    stacked = jnp.concatenate([key_rows, values], axis=1)
    labels = doc_ids + 1
    rim_kv, rim_labels = (
        extended(stacked, (("sp", 0),), WINDOW),
        extended(labels, (("sp", 0),), WINDOW),
    )
    attended = local_attention(queries, rim_kv, rim_labels, labels, sink_logits, kv_cols)
    partial_value = jnp.dot(attended, w_out, preferred_element_type=jnp.float32)
    summed = lax.psum(partial_value.astype(jnp.bfloat16), "tp").astype(jnp.float32)
    mixed = (residual.astype(jnp.float32) + summed).astype(jnp.bfloat16)
    mixed_f = mixed.astype(jnp.float32)
    mean_sq = jnp.mean(mixed_f * mixed_f, axis=1, keepdims=True)
    normed = (mixed_f * lax.rsqrt(mean_sq + EPS) * norm_gain).astype(jnp.bfloat16)
    own_cols = lax.dynamic_slice_in_dim(mixed, first_col, span_cols, 1)
    value_f32 = jnp.dot(
        normed,
        lax.all_gather(w_value_up, "sp", axis=0, tiled=True),
        preferred_element_type=jnp.float32,
    )
    gate_f32 = jnp.dot(
        normed,
        lax.all_gather(w_gate_up, "sp", axis=0, tiled=True),
        preferred_element_type=jnp.float32,
    )
    up_value = value_f32.astype(jnp.bfloat16)
    up_gate = gate_f32.astype(jnp.bfloat16)
    rim_value = extended(up_value, (("sp", 0),), 1).astype(jnp.float32)
    prev_same = (rim_labels[WINDOW - 1 : WINDOW - 1 + rows_here] == labels)[:, None]
    next_same = (rim_labels[WINDOW + 1 : WINDOW + 1 + rows_here] == labels)[:, None]
    tap_f = conv_taps.astype(jnp.float32)
    conv = (
        tap_f[0] * jnp.where(prev_same, rim_value[:-2], 0.0)
        + tap_f[1] * up_value.astype(jnp.float32)
        + tap_f[2] * jnp.where(next_same, rim_value[2:], 0.0)
    )
    hidden = (jax.nn.silu(conv) * up_gate.astype(jnp.float32)).astype(jnp.bfloat16)
    partial_down = lax.dot_general(
        hidden,
        lax.all_gather(w_down_t, "sp", axis=0, tiled=True),
        (((1,), (1,)), ((), ())),
        preferred_element_type=jnp.float32,
    )
    ffn_cols = lax.psum_scatter(
        partial_down.astype(jnp.bfloat16), "tp", scatter_dimension=1, tiled=True
    ).astype(jnp.float32)
    return (own_cols.astype(jnp.float32) + ffn_cols).astype(jnp.bfloat16)


def solution(mesh):
    placed = (
        P("sp", "tp"),
        P("sp", "tp"),
        P("sp", "tp"),
        P("tp"),
        P("sp"),
        P("sp", None),
        P("tp", None),
        P(),
        P("sp", "tp"),
        P("sp", "tp"),
        P(None, "tp"),
        P("sp", "tp"),
    )
    return jax.shard_map(
        per_device, mesh=mesh, in_specs=placed, out_specs=P("sp", "tp"), check_vma=False
    )
```

profile of v0, /device:TPU:0, one launch (start us, length us, event | category | flops | bytes accessed | tf_op | source)
XLA Modules:
  0.0 392.3 jit_solution(13465538097866399492)
XLA Ops:
  7.4 0.0 copy-start
  7.4 0.0 all-reduce.2.cloned.1.call-start
  7.4 0.8 fusion.27
  8.2 4.9 %collective-permute-start.2 = (s32[128]{0:T(128)S(1)}, s32[128]{0:T(128)S(1)}, u32[]{:S(2)}, u32[]{:S(2)}) collective-permute-start(s32[128]{0:T(128)S(1)} %get-tuple-element.22), channel_id=1, source_target_pairs={{0,4},{4,8},{8,12},{12,16},{16,20},{20,24},{24,28},{1,5},{5,9},{9,... | collective-permute-start | bytes 1544 | tf_op jit(solution)/shard_map/ppermute | solution.py:17
  13.1 1.3 collective-permute-start.3
  14.4 1.0 constant_dynamic-update-slice_fusion.1
  15.4 1.0 constant_dynamic-update-slice_fusion
  16.3 4.5 %collective-permute-start = (bf16[128,256]{1,0:T(8,128)(2,1)S(1)}, bf16[128,256]{1,0:T(8,128)(2,1)S(1)}, u32[]{:S(2)}, u32[]{:S(2)}) collective-permute-start(bf16[128,256]{1,0:T(8,128)(2,1)S(1)} %get-tuple-element.16), channel_id=1, source_target_pairs={{0,4},{4,8},{8,12},{12,16},{16,20},{20,24},{24,28},{1,5},{5,9},{9,... | collective-permute-start | bytes 196616 | tf_op jit(solution)/shard_map/ppermute | solution.py:17
  20.9 1.3 collective-permute-start.1
  22.2 0.1 abs_compare_fusion
  22.3 0.2 copy.19
  22.6 3.6 reshape.95
  26.2 0.7 max.17
  26.9 0.0 collective-permute-done.2
  26.9 0.0 collective-permute-done.3
  27.0 0.5 compare_and_fusion
  27.5 0.0 collective-permute-done
  27.5 0.0 collective-permute-done.1
  27.5 0.9 pad_maximum_fusion.2
  28.4 1.2 copy.18
  29.6 1.9 copy.20
  31.6 0.0 copy-start.1
  31.6 1.3 pad_maximum_fusion
  32.8 0.1 fusion.29
  33.0 0.1 copy-done.1
  33.1 1.8 fusion
  34.9 0.1 broadcast_maximum_fusion
  34.9 2.3 fusion.3
  37.3 0.1 exponential_add_fusion
  37.4 2.8 fusion.17
  40.1 0.6 copy.24
  40.7 0.0 copy-done
  40.7 3.5 convolution_convert_fusion
  44.2 0.0 all-reduce.2.cloned.1.call-update
  44.2 0.0 all-gather.4.cloned.1.call-start
  44.2 0.5 all-gather.4.cloned.1.call-update
  44.8 0.0 all-gather.6.cloned.1.call-start
  44.8 0.5 all-gather.6.cloned.1.call-update
  45.4 0.0 all-gather.8.cloned.1.call-start
  45.4 0.5 all-gather.8.cloned.1.call-update
  45.9 0.2 reduce-scatter.2.cloned.1.call-start
  46.2 0.0 copy-done.4
  46.2 0.1 slice_reduce_fusion.2
  46.3 0.0 copy-start.5
  46.3 69.8 %all-reduce.2.cloned.1.call-done = bf16[768,2048]{1,0:T(8,128)(2,1)} async-done(((bf16[768,2048]{1,0:T(8,128)(2,1)}), bf16[768,2048]{1,0:T(8,128)(2,1)}) %all-reduce.2.cloned.1.call-update) | async-done | bytes 3145744 | tf_op jit(solution)/shard_map/psum | solution.py:82
  116.1 6.0 %fusion.4 = (f32[768]{0:T(1024)S(1)}, bf16[768,2048]{1,0:T(8,128)(2,1)}) fusion(bf16[768,2048]{1,0:T(8,128)(2,1)} %all-reduce.2.cloned.1.call-done, bf16[768,2048]{1,0:T(8,128)(2,1)} %param.17), kind=kLoop, calls=%fused_computation.9 | loop fusion | flops 11009280 | bytes 9440256 | tf_op jit(solution)/shard_map/reduce_sum | solution.py:85
  122.1 20.2 %all-gather.4.cloned.1.call-done = bf16[2048,1408]{1,0:T(8,128)(2,1)} async-done(((bf16[256,1408]{1,0:T(8,128)(2,1)}), bf16[2048,1408]{1,0:T(8,128)(2,1)}) %all-gather.4.cloned.1.call-update) | async-done | bytes 5767184 | tf_op jit(solution)/shard_map/all_gather | solution.py:90
  142.3 0.0 copy-done.5
  142.3 8.6 %convolution_convert_fusion.3 = bf16[768,1408]{1,0:T(8,128)(2,1)S(1)} fusion(bf16[2048,1408]{1,0:T(8,128)(2,1)} %all-gather.4.cloned.1.call-done, bf16[768,2048]{1,0:T(8,128)(2,1)} %get-tuple-element.9, f32[2048]{0:T(1024)S(1)} %copy-done.5, f32[768]{0:T(1024)S(1)} %add_rsqrt_fusion), kind=kOutput, calls=%fused_computation.24 | convolution fusion | flops 4436557824 | bytes 11086848 | tf_op jit(solution)/shard_map/dot_general | solution.py:88
  150.9 0.0 copy-start.2
  150.9 2.4 collective-permute-start.4
  153.4 1.3 collective-permute-start.5
  154.7 0.0 copy-done.3
  154.7 0.1 slice_compare_fusion.1
  154.8 0.0 collective-permute-done.4
  154.8 4.4 %collective-permute-done.5 = bf16[1,1408]{1,0:T(2,128)(2,1)S(1)} collective-permute-done((bf16[1,1408]{1,0:T(2,128)(2,1)S(1)}, bf16[1,1408]{1,0:T(2,128)(2,1)S(1)}, u32[]{:S(2)}, u32[]{:S(2)}) %collective-permute-start.5) | collective-permute-done | bytes 2848 | tf_op jit(solution)/shard_map/ppermute | solution.py:20
  159.1 0.0 copy-done.2
  159.1 2.5 maximum_convert_fusion
  161.7 73.1 %all-gather.6.cloned.1.call-done = bf16[2048,1408]{1,0:T(8,128)(2,1)} async-done(((bf16[256,1408]{1,0:T(8,128)(2,1)}), bf16[2048,1408]{1,0:T(8,128)(2,1)}) %all-gather.6.cloned.1.call-update) | async-done | bytes 5767184 | tf_op jit(solution)/shard_map/all_gather | solution.py:95
  234.8 92.3 %all-gather.8.cloned.1.call-done = bf16[2048,1408]{1,0:T(8,128)(2,1)} async-done(((bf16[256,1408]{1,0:T(8,128)(2,1)}), bf16[2048,1408]{1,0:T(8,128)(2,1)}) %all-gather.8.cloned.1.call-update) | async-done | bytes 5767184 | tf_op jit(solution)/shard_map/all_gather | solution.py:112
  327.1 19.1 %convolution_convert_fusion.1 = bf16[768,2048]{1,0:T(8,128)(2,1)} fusion(bf16[2048,1408]{1,0:T(8,128)(2,1)} %all-gather.8.cloned.1.call-done, f32[770,1408]{1,0:T(8,128)} %maximum_convert_fusion, bf16[768,1408]{1,0:T(8,128)(2,1)} %copy-done.2, f32[1408]{0:T(1024)S(1)} %get-tuple-element.6, f32[1408]{0:T(1024)S(1)} %get-tuple-element.7, ...), kind=kOutput, calls=%fused_computation.22 | convolution fusion | flops 8883535872 | bytes 28668928 | tf_op jit(solution)/shard_map/dot_general | solution.py:110
  346.2 0.0 reduce-scatter.2.cloned.1.call-update
  346.3 36.0 %reduce-scatter.2.cloned.1.call-done = bf16[768,512]{1,0:T(8,128)(2,1)} async-done(((bf16[768,2048]{1,0:T(8,128)(2,1)}), bf16[768,512]{1,0:T(8,128)(2,1)}) %reduce-scatter.2.cloned.1.call-update) | async-done | bytes 786448 | tf_op jit(solution)/shard_map/reduce_scatter | solution.py:116
  382.3 2.5 add_convert_fusion.1
  (11 shorter events, 0.1 us)
Async XLA Ops:
  7.4 33.3 %copy-start = (bf16[512,2048]{1,0:T(8,128)(2,1)S(1)}, bf16[512,2048]{1,0:T(8,128)(2,1)}, u32[]{:S(2)}) copy-start(bf16[512,2048]{1,0:T(8,128)(2,1)} %param.18) | copy-start | bytes 6291460
  7.4 108.7 %all-reduce.2.cloned.1.call-start = ((), (), s32[]{:S(2)}) async-start(), calls=%async_computation.1 | async-start | bytes 6291456 | tf_op jit(solution)/shard_map/psum | solution.py:82
  8.2 18.7 %collective-permute-start.2 = (s32[128]{0:T(128)S(1)}, s32[128]{0:T(128)S(1)}, u32[]{:S(2)}, u32[]{:S(2)}) collective-permute-start(s32[128]{0:T(128)S(1)} %get-tuple-element.22), channel_id=1, source_target_pairs={{0,4},{4,8},{8,12},{12,16},{16,20},{20,24},{24,28},{1,5},{5,9},{9,... | collective-permute-start | bytes 1544 | tf_op jit(solution)/shard_map/ppermute | solution.py:17
  13.1 13.9 %collective-permute-start.3 = (s32[128]{0:T(128)S(1)}, s32[128]{0:T(128)S(1)}, u32[]{:S(2)}, u32[]{:S(2)}) collective-permute-start(s32[128]{0:T(128)S(1)} %get-tuple-element.23), channel_id=1, source_target_pairs={{4,0},{8,4},{12,8},{16,12},{20,16},{24,20},{28,24},{5,1},{9,5},{13... | collective-permute-start | bytes 1544 | tf_op jit(solution)/shard_map/ppermute | solution.py:20
  16.3 11.1 %collective-permute-start = (bf16[128,256]{1,0:T(8,128)(2,1)S(1)}, bf16[128,256]{1,0:T(8,128)(2,1)S(1)}, u32[]{:S(2)}, u32[]{:S(2)}) collective-permute-start(bf16[128,256]{1,0:T(8,128)(2,1)S(1)} %get-tuple-element.16), channel_id=1, source_target_pairs={{0,4},{4,8},{8,12},{12,16},{16,20},{20,24},{24,28},{1,5},{5,9},{9,... | collective-permute-start | bytes 196616 | tf_op jit(solution)/shard_map/ppermute | solution.py:17
  20.9 6.6 %collective-permute-start.1 = (bf16[128,256]{1,0:T(8,128)(2,1)S(1)}, bf16[128,256]{1,0:T(8,128)(2,1)S(1)}, u32[]{:S(2)}, u32[]{:S(2)}) collective-permute-start(bf16[128,256]{1,0:T(8,128)(2,1)S(1)} %get-tuple-element.17), channel_id=1, source_target_pairs={{4,0},{8,4},{12,8},{16,12},{20,16},{24,20},{28,24},{5,1},{9,5},{13... | collective-permute-start | bytes 196616 | tf_op jit(solution)/shard_map/ppermute | solution.py:20
  31.6 1.5 copy-start.1
  44.2 2.0 copy-start.4
  44.2 98.1 %all-gather.4.cloned.1.call-start = ((), (), s32[]{:S(2)}) async-start(), calls=%async_computation.2 | async-start | bytes 6488064 | tf_op jit(solution)/shard_map/all_gather | solution.py:90
  44.8 190.0 %all-gather.6.cloned.1.call-start = ((), (), s32[]{:S(2)}) async-start(), calls=%async_computation.3 | async-start | bytes 6488064 | tf_op jit(solution)/shard_map/all_gather | solution.py:95
  45.4 281.8 %all-gather.8.cloned.1.call-start = ((), (), s32[]{:S(2)}) async-start(), calls=%async_computation.4 | async-start | bytes 6488064 | tf_op jit(solution)/shard_map/all_gather | solution.py:112
  45.9 336.3 %reduce-scatter.2.cloned.1.call-start = ((), (), s32[]{:S(2)}) async-start(), calls=%async_computation.5 | async-start | bytes 3932160 | tf_op jit(solution)/shard_map/reduce_scatter | solution.py:116
  46.3 96.0 %copy-start.5 = (f32[2048]{0:T(1024)S(1)}, f32[2048]{0:T(1024)}, u32[]{:S(2)}) copy-start(f32[2048]{0:T(1024)} %param.19) | copy-start | bytes 24580
  142.3 12.4 %copy-start.3 = (s32[768]{0:T(1024)S(1)}, s32[768]{0:T(1024)}, u32[]{:S(2)}) copy-start(s32[768]{0:T(1024)} %param.16) | copy-start | bytes 9220
  150.9 8.2 %copy-start.2 = (bf16[768,1408]{1,0:T(8,128)(2,1)}, bf16[768,1408]{1,0:T(8,128)(2,1)S(1)}, u32[]{:S(2)}) copy-start(bf16[768,1408]{1,0:T(8,128)(2,1)S(1)} %convolution_convert_fusion.3) | copy-start | bytes 6488068
  150.9 3.8 collective-permute-start.4
  153.4 5.8 %collective-permute-start.5 = (bf16[1,1408]{1,0:T(2,128)(2,1)S(1)}, bf16[1,1408]{1,0:T(2,128)(2,1)S(1)}, u32[]{:S(2)}, u32[]{:S(2)}) collective-permute-start(bf16[1,1408]{1,0:T(2,128)(2,1)S(1)} %get-tuple-element.11), channel_id=1, source_target_pairs={{4,0},{8,4},{12,8},{16,12},{20,16},{24,20},{28,24},{5,1},{9,5},{13... | collective-permute-start | bytes 8456 | tf_op jit(solution)/shard_map/ppermute | solution.py:20
Sparse Core Ops, SparseCore 0:
  44.3 71.7 all-reduce.1
  346.4 35.8 reduce-scatter.1
Sparse Core Ops, SparseCore 1:
  46.9 95.4 all-gather.3
  144.4 90.4 all-gather.5
  236.8 90.2 all-gather.7
where the time goes:
time: 393 us; the launch traced here: 392 us
  waiting for transfers between devices  297 us (76%)
  matrix products  35.7 us (9%)
  other arithmetic  17.2 us (4%)
  starting transfers between devices  16.1 us (4%)
  between operations  15.3 us (4%)
  local copies, waits for them, and re-layouts  10.6 us (3%)
    all_gather x1, waiting for transfers between devices, per_device(): lax.all_gather(w_down_t, 'sp', axis=0, tiled=True)  92.3 us
    all_gather x1, waiting for transfers between devices, per_device(): lax.all_gather(w_gate_up, 'sp', axis=0, tiled=True)  73.1 us
    psum x1, waiting for transfers between devices, per_device(): lax.psum(partial_value.astype(jnp.bfloat16), 'tp').astype(jnp.float32)  69.8 us
    reduce_scatter x1, waiting for transfers between devices, per_device(): lax.psum_scatter(partial_down.astype(jnp.bfloat16), 'tp', scatter_dimensi...  36 us
    all_gather x1, waiting for transfers between devices, per_device(): lax.all_gather(w_value_up, 'sp', axis=0, tiled=True)  20.2 us
    dot_general x1, matrix products, per_device(): lax.dot_general(hidden, lax.all_gather(w_down_t, 'sp', axis=0, tiled=True...  19.1 us
    ppermute x3, starting transfers between devices, extended(): lax.ppermute(lax.slice_in_dim(block, block.shape[dim] - width, None, axis...  11.9 us
    dot_general x1, matrix products, per_device(): jnp.dot(normed, lax.all_gather(w_value_up, 'sp', axis=0, tiled=True), pre...  8.59 us
  transfers between devices with their start and end apart: 11, of which 6 were waited for; matrix products, arithmetic and copies ran while one was open for 6% of the time, Pallas kernels for 0%

commit v1 on v0

--- a/solution.py
+++ b/solution.py
@@ -79,7 +79,9 @@
     )
     attended = local_attention(queries, rim_kv, rim_labels, labels, sink_logits, kv_cols)
     partial_value = jnp.dot(attended, w_out, preferred_element_type=jnp.float32)
-    summed = lax.psum(partial_value.astype(jnp.bfloat16), "tp").astype(jnp.float32)
+    summed = jnp.sum(lax.all_gather(partial_value.astype(jnp.bfloat16), "tp"), axis=0).astype(
+        jnp.float32
+    )
     mixed = (residual.astype(jnp.float32) + summed).astype(jnp.bfloat16)
     mixed_f = mixed.astype(jnp.float32)
     mean_sq = jnp.mean(mixed_f * mixed_f, axis=1, keepdims=True)

time: 393 us -> 474 us (1.21)
  waiting for transfers between devices: 297 us -> 369 us
  other arithmetic: 17.2 us -> 27.6 us
    all_gather x0 -> x1, waiting for transfers between devices: none -> 83.1 us  [per_device(): lax.all_gather(partial_value.astype(jnp.bfloat16), 'tp')]
    psum x1 -> x0, waiting for transfers between devices: 69.8 us -> none  [per_device(): lax.psum(partial_value.astype(jnp.bfloat16), 'tp').astype(jnp.float32)]
    all_gather x1, waiting for transfers between devices: 20.2 us -> 78.1 us  [per_device(): lax.all_gather(w_value_up, 'sp', axis=0, tiled=True)]
    all_gather x1, waiting for transfers between devices: 73.1 us -> 92.6 us  [per_device(): lax.all_gather(w_gate_up, 'sp', axis=0, tiled=True)]
    all_gather x1, waiting for transfers between devices: 92.3 us -> 73.5 us  [per_device(): lax.all_gather(w_down_t, 'sp', axis=0, tiled=True)]
    reduce_sum x0 -> x1, other arithmetic: none -> 10.2 us  [per_device(): jnp.sum(lax.all_gather(partial_value.astype(jnp.bfloat16), 'tp'), axis=0)]
  transfers between devices with their start and end apart: 11 -> 11, of which waited for: 6 -> 6; matrix products, arithmetic and copies ran while one was open for 6% -> 7% of each run, Pallas kernels for 0% -> 0%
where the time goes in v1:
time: 474 us; the launch traced here: 473 us
  waiting for transfers between devices  369 us (78%)
  matrix products  35.8 us (8%)
  other arithmetic  27.6 us (6%)
  starting transfers between devices  16.3 us (3%)
  between operations  13.4 us (3%)
  local copies, waits for them, and re-layouts  10.6 us (2%)
    all_gather x1, waiting for transfers between devices, per_device(): lax.all_gather(w_gate_up, 'sp', axis=0, tiled=True)  92.6 us
    all_gather x1, waiting for transfers between devices, per_device(): lax.all_gather(partial_value.astype(jnp.bfloat16), 'tp')  83.1 us
    all_gather x1, waiting for transfers between devices, per_device(): lax.all_gather(w_value_up, 'sp', axis=0, tiled=True)  78.1 us
    all_gather x1, waiting for transfers between devices, per_device(): lax.all_gather(w_down_t, 'sp', axis=0, tiled=True)  73.5 us
    reduce_scatter x1, waiting for transfers between devices, per_device(): lax.psum_scatter(partial_down.astype(jnp.bfloat16), 'tp', scatter_dimensi...  36 us
    dot_general x1, matrix products, per_device(): lax.dot_general(hidden, lax.all_gather(w_down_t, 'sp', axis=0, tiled=True...  19.2 us
    ppermute x3, starting transfers between devices, extended(): lax.ppermute(lax.slice_in_dim(block, block.shape[dim] - width, None, axis...  11.9 us
    reduce_sum x1, other arithmetic, per_device(): jnp.sum(lax.all_gather(partial_value.astype(jnp.bfloat16), 'tp'), axis=0)  10.2 us
  transfers between devices with their start and end apart: 11, of which 6 were waited for; matrix products, arithmetic and copies ran while one was open for 7% of the time, Pallas kernels for 0%

profile of v1, /device:TPU:0, one launch (start us, length us, event | category | flops | bytes accessed | tf_op | source)
XLA Modules:
  0.0 473.1 jit_solution(17691840130367883979)
XLA Ops:
  6.5 0.0 copy-start
  6.5 0.0 all-gather.12.cloned.1.call-start
  6.5 0.8 fusion.27
  7.4 4.9 %collective-permute-start.2 = (s32[128]{0:T(128)S(1)}, s32[128]{0:T(128)S(1)}, u32[]{:S(2)}, u32[]{:S(2)}) collective-permute-start(s32[128]{0:T(128)S(1)} %get-tuple-element.22), channel_id=1, source_target_pairs={{0,4},{4,8},{8,12},{12,16},{16,20},{20,24},{24,28},{1,5},{5,9},{9,... | collective-permute-start | bytes 1544 | tf_op jit(solution)/shard_map/ppermute | solution.py:17
  12.3 1.3 collective-permute-start.3
  13.6 1.0 constant_dynamic-update-slice_fusion.1
  14.5 1.0 constant_dynamic-update-slice_fusion
  15.5 4.5 collective-permute-start
  20.1 1.3 collective-permute-start.1
  21.4 0.1 abs_compare_fusion
  21.5 0.2 copy.19
  21.7 3.6 reshape.96
  25.4 0.7 max.17
  26.1 0.0 collective-permute-done.2
  26.1 0.0 collective-permute-done.3
  26.2 0.5 compare_and_fusion
  26.7 0.0 collective-permute-done
  26.7 0.0 collective-permute-done.1
  26.7 0.9 pad_maximum_fusion.2
  27.6 1.2 copy.18
  28.8 1.9 copy.20
  30.7 1.3 pad_maximum_fusion
  32.0 0.1 fusion.29
  32.2 0.1 copy-done.2
  32.3 1.8 fusion
  34.0 0.1 broadcast_maximum_fusion
  34.1 2.3 fusion.3
  36.4 0.1 exponential_add_fusion
  36.5 2.8 fusion.17
  39.3 0.6 copy.24
  39.9 0.0 copy-done
  39.9 3.5 convolution_convert_fusion
  43.3 0.0 all-gather.12.cloned.1.call-update
  43.4 0.0 all-gather.6.cloned.1.call-start
  43.4 0.7 all-gather.6.cloned.1.call-update
  44.1 0.0 all-gather.10.cloned.1.call-start
  44.2 0.7 all-gather.10.cloned.1.call-update
  44.8 0.0 all-gather.8.cloned.1.call-start
  44.9 0.5 all-gather.8.cloned.1.call-update
  45.4 0.2 reduce-scatter.2.cloned.1.call-start
  45.6 0.0 copy-done.5
  45.7 0.1 slice_reduce_fusion.2
  45.7 83.1 %all-gather.12.cloned.1.call-done = bf16[3072,2048]{1,0:T(8,128)(2,1)} async-done(((bf16[768,2048]{1,0:T(8,128)(2,1)}), bf16[3072,2048]{1,0:T(8,128)(2,1)}) %all-gather.12.cloned.1.call-update) | async-done | bytes 12582928 | tf_op jit(solution)/shard_map/all_gather | solution.py:82
  128.9 10.2 %reduce_sum.31 = bf16[768,2048]{1,0:T(8,128)(2,1)} reduce(bf16[4,768,2048]{2,1,0:T(8,128)(2,1)} %bitcast.53, bf16[]{:T(256)} %constant.12.clone.1), dimensions={0}, to_apply=%region_2.3 | reduce | flops 4718592 | bytes 15728642 | tf_op jit(solution)/shard_map/reduce_sum | solution.py:82
  139.1 6.2 %fusion.4 = (f32[768]{0:T(1024)S(1)}, bf16[768,2048]{1,0:T(8,128)(2,1)}) fusion(bf16[768,2048]{1,0:T(8,128)(2,1)} %reduce_sum.31, bf16[768,2048]{1,0:T(8,128)(2,1)} %param.17), kind=kLoop, calls=%fused_computation.9 | loop fusion | flops 11009280 | bytes 9440256 | tf_op jit(solution)/shard_map/reduce_sum | solution.py:87
  145.3 78.1 %all-gather.6.cloned.1.call-done = bf16[2048,1408]{1,0:T(8,128)(2,1)} async-done(((bf16[256,1408]{1,0:T(8,128)(2,1)}), bf16[2048,1408]{1,0:T(8,128)(2,1)}) %all-gather.6.cloned.1.call-update) | async-done | bytes 5767184 | tf_op jit(solution)/shard_map/all_gather | solution.py:92
  223.4 0.0 copy-done.6
  223.4 8.6 %convolution_convert_fusion.3 = bf16[768,1408]{1,0:T(8,128)(2,1)S(1)} fusion(bf16[2048,1408]{1,0:T(8,128)(2,1)} %all-gather.6.cloned.1.call-done, bf16[768,2048]{1,0:T(8,128)(2,1)} %get-tuple-element.9, f32[2048]{0:T(1024)S(1)} %copy-done.6, f32[768]{0:T(1024)S(1)} %add_rsqrt_fusion), kind=kOutput, calls=%fused_computation.24 | convolution fusion | flops 4436557824 | bytes 11086848 | tf_op jit(solution)/shard_map/dot_general | solution.py:90
  232.0 0.0 copy-start.3
  232.0 2.5 collective-permute-start.4
  234.5 1.5 collective-permute-start.5
  236.0 0.0 copy-done.4
  236.0 0.1 slice_compare_fusion.1
  236.1 0.0 collective-permute-done.4
  236.1 4.2 collective-permute-done.5
  240.2 0.0 copy-done.3
  240.2 2.4 maximum_convert_fusion
  242.7 73.5 %all-gather.10.cloned.1.call-done = bf16[2048,1408]{1,0:T(8,128)(2,1)} async-done(((bf16[256,1408]{1,0:T(8,128)(2,1)}), bf16[2048,1408]{1,0:T(8,128)(2,1)}) %all-gather.10.cloned.1.call-update) | async-done | bytes 5767184 | tf_op jit(solution)/shard_map/all_gather | solution.py:114
  316.2 92.6 %all-gather.8.cloned.1.call-done = bf16[2048,1408]{1,0:T(8,128)(2,1)} async-done(((bf16[256,1408]{1,0:T(8,128)(2,1)}), bf16[2048,1408]{1,0:T(8,128)(2,1)}) %all-gather.8.cloned.1.call-update) | async-done | bytes 5767184 | tf_op jit(solution)/shard_map/all_gather | solution.py:97
  408.8 19.2 %convolution_convert_fusion.1 = bf16[768,2048]{1,0:T(8,128)(2,1)} fusion(bf16[2048,1408]{1,0:T(8,128)(2,1)} %all-gather.10.cloned.1.call-done, f32[770,1408]{1,0:T(8,128)} %maximum_convert_fusion, bf16[768,1408]{1,0:T(8,128)(2,1)} %copy-done.3, f32[1408]{0:T(1024)S(1)} %get-tuple-element.6, f32[1408]{0:T(1024)S(1)} %get-tuple-element.7, ...), kind=kOutput, calls=%fused_computation.22 | convolution fusion | flops 8883535872 | bytes 28668928 | tf_op jit(solution)/shard_map/dot_general | solution.py:112
  428.0 0.0 reduce-scatter.2.cloned.1.call-update
  428.1 36.0 %reduce-scatter.2.cloned.1.call-done = bf16[768,512]{1,0:T(8,128)(2,1)} async-done(((bf16[768,2048]{1,0:T(8,128)(2,1)}), bf16[768,512]{1,0:T(8,128)(2,1)}) %reduce-scatter.2.cloned.1.call-update) | async-done | bytes 786448 | tf_op jit(solution)/shard_map/reduce_scatter | solution.py:118
  464.1 2.5 add_convert_fusion.1
  466.6 0.0 copy-done.1
  (14 shorter events, 0.1 us)
Async XLA Ops:
  6.5 33.3 %copy-start = (bf16[512,2048]{1,0:T(8,128)(2,1)S(1)}, bf16[512,2048]{1,0:T(8,128)(2,1)}, u32[]{:S(2)}) copy-start(bf16[512,2048]{1,0:T(8,128)(2,1)} %param.18) | copy-start | bytes 6291460
  6.5 122.3 %all-gather.12.cloned.1.call-start = ((), (), s32[]{:S(2)}) async-start(), calls=%async_computation.5 | async-start | bytes 15728640 | tf_op jit(solution)/shard_map/all_gather | solution.py:82
  7.4 18.7 %collective-permute-start.2 = (s32[128]{0:T(128)S(1)}, s32[128]{0:T(128)S(1)}, u32[]{:S(2)}, u32[]{:S(2)}) collective-permute-start(s32[128]{0:T(128)S(1)} %get-tuple-element.22), channel_id=1, source_target_pairs={{0,4},{4,8},{8,12},{12,16},{16,20},{20,24},{24,28},{1,5},{5,9},{9,... | collective-permute-start | bytes 1544 | tf_op jit(solution)/shard_map/ppermute | solution.py:17
  12.3 13.9 %collective-permute-start.3 = (s32[128]{0:T(128)S(1)}, s32[128]{0:T(128)S(1)}, u32[]{:S(2)}, u32[]{:S(2)}) collective-permute-start(s32[128]{0:T(128)S(1)} %get-tuple-element.23), channel_id=1, source_target_pairs={{4,0},{8,4},{12,8},{16,12},{20,16},{24,20},{28,24},{5,1},{9,5},{13... | collective-permute-start | bytes 1544 | tf_op jit(solution)/shard_map/ppermute | solution.py:20
  15.5 11.1 %collective-permute-start = (bf16[128,256]{1,0:T(8,128)(2,1)S(1)}, bf16[128,256]{1,0:T(8,128)(2,1)S(1)}, u32[]{:S(2)}, u32[]{:S(2)}) collective-permute-start(bf16[128,256]{1,0:T(8,128)(2,1)S(1)} %get-tuple-element.16), channel_id=1, source_target_pairs={{0,4},{4,8},{8,12},{12,16},{16,20},{20,24},{24,28},{1,5},{5,9},{9,... | collective-permute-start | bytes 196616 | tf_op jit(solution)/shard_map/ppermute | solution.py:17
  20.1 6.6 %collective-permute-start.1 = (bf16[128,256]{1,0:T(8,128)(2,1)S(1)}, bf16[128,256]{1,0:T(8,128)(2,1)S(1)}, u32[]{:S(2)}, u32[]{:S(2)}) collective-permute-start(bf16[128,256]{1,0:T(8,128)(2,1)S(1)} %get-tuple-element.17), channel_id=1, source_target_pairs={{4,0},{8,4},{12,8},{16,12},{20,16},{24,20},{28,24},{5,1},{9,5},{13... | collective-permute-start | bytes 196616 | tf_op jit(solution)/shard_map/ppermute | solution.py:20
  30.7 1.5 copy-start.2
  43.3 2.3 copy-start.5
  43.4 180.0 %all-gather.6.cloned.1.call-start = ((), (), s32[]{:S(2)}) async-start(), calls=%async_computation.1 | async-start | bytes 6488064 | tf_op jit(solution)/shard_map/all_gather | solution.py:92
  44.1 272.1 %all-gather.10.cloned.1.call-start = ((), (), s32[]{:S(2)}) async-start(), calls=%async_computation.3 | async-start | bytes 6488064 | tf_op jit(solution)/shard_map/all_gather | solution.py:114
  44.8 363.9 %all-gather.8.cloned.1.call-start = ((), (), s32[]{:S(2)}) async-start(), calls=%async_computation.2 | async-start | bytes 6488064 | tf_op jit(solution)/shard_map/all_gather | solution.py:97
  45.4 418.7 %reduce-scatter.2.cloned.1.call-start = ((), (), s32[]{:S(2)}) async-start(), calls=%async_computation.4 | async-start | bytes 3932160 | tf_op jit(solution)/shard_map/reduce_scatter | solution.py:118
  139.1 84.3 %copy-start.6 = (f32[2048]{0:T(1024)S(1)}, f32[2048]{0:T(1024)}, u32[]{:S(2)}) copy-start(f32[2048]{0:T(1024)} %param.19) | copy-start | bytes 24580
  223.4 12.6 %copy-start.4 = (s32[768]{0:T(1024)S(1)}, s32[768]{0:T(1024)}, u32[]{:S(2)}) copy-start(s32[768]{0:T(1024)} %param.16) | copy-start | bytes 9220
  232.0 8.3 %copy-start.3 = (bf16[768,1408]{1,0:T(8,128)(2,1)}, bf16[768,1408]{1,0:T(8,128)(2,1)S(1)}, u32[]{:S(2)}) copy-start(bf16[768,1408]{1,0:T(8,128)(2,1)S(1)} %convolution_convert_fusion.3) | copy-start | bytes 6488068
  232.0 4.1 collective-permute-start.4
  234.5 5.8 %collective-permute-start.5 = (bf16[1,1408]{1,0:T(2,128)(2,1)S(1)}, bf16[1,1408]{1,0:T(2,128)(2,1)S(1)}, u32[]{:S(2)}, u32[]{:S(2)}) collective-permute-start(bf16[1,1408]{1,0:T(2,128)(2,1)S(1)} %get-tuple-element.11), channel_id=1, source_target_pairs={{4,0},{8,4},{12,8},{16,12},{20,16},{24,20},{28,24},{5,1},{9,5},{13... | collective-permute-start | bytes 8456 | tf_op jit(solution)/shard_map/ppermute | solution.py:20
  408.8 57.8 %copy-start.1 = (bf16[512,2048]{1,0:T(8,128)(2,1)S(1)}, bf16[512,2048]{1,0:T(8,128)(2,1)}, u32[]{:S(2)}) copy-start(bf16[512,2048]{1,0:T(8,128)(2,1)} %param.18) | copy-start | bytes 6291460
Sparse Core Ops, SparseCore 0:
  43.5 85.3 all-gather.11
  131.1 92.2 all-gather.5
  225.6 90.5 all-gather.9
  318.3 90.4 all-gather.7
  428.2 35.8 reduce-scatter.1
